TPU v7x, 512 devices: a 8x2x16 block of a 8x8x16 slice. The times are simulated.
512 devices in a mesh: grp: 2 (over y), sp: 32 (over z, core), tp: 8 (over x).
Axes of the slice: x: 8, y: 2, z: 16, core: 2. Of those that a mesh axis runs over, the one named last changes fastest.
The devices are a block of a 8x8x16 slice.
Arguments:
- residual: bfloat16 [16384, 2048], P(('grp', 'sp')), parts along dimension 0, may hold values from -34 to 34
- queries: bfloat16 [16384, 1024], P(('grp', 'sp'), 'tp'), parts along dimension 0, may hold values from -400 to 400
- keys: bfloat16 [16384, 512], P(('grp', 'sp'), 'tp'), parts along dimension 0, may hold values from -8 to 8
- values: bfloat16 [16384, 512], P(('grp', 'sp'), 'tp'), parts along dimension 0, may hold values from -6 to 6
- segments: int32 [16384], P(('grp', 'sp')), parts along dimension 0, may hold values from 0 to 16, never falling along the last dimension, each value on 1 to 768 neighbouring positions
- routes: int32 [16384, 2], P(('grp', 'sp')), parts along dimension 0, may hold values from 0 to 31, all different within a row; in each aligned block of 256 rows (0 to 255, 256 to 511, ...) at most 32 rows name the same one
- route_weight: float32 [16384, 2], P(('grp', 'sp')), parts along dimension 0, may hold values from 0.3 to 3
- sinks: float32 [16], P('tp'), may hold values from 1 to 6
- out_weight: bfloat16 [1024, 2048], P('tp'), may hold values from -1 to 1
- norm_gain: float32 [2048], replicated, may hold values from 0.1 to 1.9
- expert_gate: bfloat16 [32, 2048, 1024], P('sp', None, 'tp'), may hold values from -0.125 to 0.125
- expert_up: bfloat16 [32, 2048, 1024], P('sp', None, 'tp'), may hold values from -0.125 to 0.125
- expert_down: bfloat16 [32, 1024, 2048], P('sp', None, 'tp'), may hold values from -0.1875 to 0.1875
- shared_gate: bfloat16 [2048, 1024], P(None, 'tp'), may hold values from -0.125 to 0.125
- shared_up: bfloat16 [2048, 1024], P(None, 'tp'), may hold values from -0.125 to 0.125
- shared_down: bfloat16 [1024, 2048], P(None, 'tp'), may hold values from -0.1875 to 0.1875
Outputs:
- mixed: bfloat16 [16384, 2048], P(('grp', 'sp'), 'tp'), parts along dimension 0
There are 2 independent parts, one for each index of `grp`. A program takes and returns all parts, laid end to end along the dimension named above; an argument that names none is the same for every part. Nothing has to cross between parts.
Inputs may be any that keep to these rules, and one draw needn't show every extreme that they name: `routes`: each row names 2 different experts. In the rows of one device no expert is named by more than 32 rows, and in some device's rows an expert is named by exactly 32. `segments`: document numbers never fall along the positions; every document spans 1 to 768 positions and one spans exactly 768.
All inputs are finite; a program needn't handle non-finite values.
Results may differ from a plain program's by a relative error of at most 0.0065.
Values may be sent and summed in bfloat16 or wider, within the bound.
A program may use at most 64 MiB of HBM per device.

v0:
```python
import jax
import jax.numpy as jnp
from jax import lax
from jax.sharding import Mesh
from jax.sharding import PartitionSpec as P

HEAD_DIM = 64
WINDOW = 128
SP = ("sp_0", "sp_1")
GRP_SP = ("grp", "sp_0", "sp_1")
epsilon = 1e-06


def passed_along(value, axis, steps):
    count = lax.axis_size(axis)
    leading, last = (max(0, -steps), min(count, count - steps))
    return lax.ppermute(value, axis, [(source, source + steps) for source in range(leading, last)])


def split_up(array, dim, size):
    shape = array.shape
    blocks = array.reshape(*shape[:dim], size, shape[dim] // size, *shape[dim + 1 :])
    return jnp.moveaxis(blocks, dim, 0)


def sent_and_summed(array, axis, dim):
    size = lax.axis_size(axis)
    blocks = lax.all_to_all(split_up(array, dim, size), axis, 0, 0, tiled=True)
    return jnp.sum(blocks.astype(jnp.float32), axis=0)


def sent_to_all(array, axis):
    size = lax.axis_size(axis)
    return lax.all_to_all(
        jnp.broadcast_to(array[None], (size, *array.shape)), axis, 0, 0, tiled=True
    )


def in_order(blocks, dim):
    blocks = jnp.moveaxis(blocks, 0, dim)
    shape = blocks.shape
    return blocks.reshape(*shape[:dim], shape[dim] * shape[dim + 1], *shape[dim + 2 :])


def collect(array, axis, dim):
    blocks = sent_to_all(array, axis)
    return in_order(blocks, dim)


def moved_by_axis(blocks, axes, order):
    shape = [lax.axis_size(a) for a in axes]
    blocks = blocks.reshape(*shape, *blocks.shape[1:])
    for k in order:
        blocks = lax.all_to_all(blocks, axes[k], split_axis=k, concat_axis=k, tiled=True)
    return blocks.reshape(-1, *blocks.shape[len(axes) :])


def two_step_exchange(array, groups, order, split_dim, concat_dim):
    size = lax.axis_size(groups[0]) * lax.axis_size(groups[1])
    blocks = split_up(array, split_dim, size)
    return in_order(moved_by_axis(blocks, groups, order), concat_dim)


def sent_together(arrays, axis, dim, along):
    ends, at = ([], 0)
    for a in arrays[:-1]:
        at += a.shape[along]
        ends.append(at)
    both = jnp.concatenate(arrays, axis=along)
    return tuple(jnp.split(lax.all_gather(both, axis, axis=dim, tiled=True), ends, axis=along))


def banded(prev_rows, own_rows, window_len):
    blocks = own_rows.shape[0] // window_len
    joined = jnp.concatenate([prev_rows, own_rows], axis=0)
    shaped = joined.reshape((blocks + 1, window_len) + own_rows.shape[1:])
    return jnp.concatenate([shaped[:-1], shaped[1:]], axis=1)


def shards(
    residual,
    queries,
    keys,
    values,
    segments,
    routes,
    route_weight,
    sinks,
    out_weight,
    norm_gain,
    expert_gate,
    expert_up,
    expert_down,
    shared_gate,
    shared_up,
    shared_down,
):
    rows_here = residual.shape[0]
    model_width = residual.shape[1]
    tp_count = lax.axis_size("tp")
    tp_index = lax.axis_index("tp")
    head_local = queries.shape[1] // HEAD_DIM
    kv_local = keys.shape[1] // HEAD_DIM
    group_size = head_local // kv_local
    window_len = WINDOW
    blocks = rows_here // window_len
    own_marks = (segments % 256 + 1).astype(jnp.bfloat16)
    prev_keys, prev_values, prev_marks = passed_along(
        (
            keys[rows_here - window_len :],
            values[rows_here - window_len :],
            own_marks[rows_here - window_len :],
        ),
        SP,
        1,
    )
    key_band = banded(prev_keys, keys, window_len).reshape(
        blocks, 2 * window_len, kv_local, HEAD_DIM
    )
    value_band = banded(prev_values, values, window_len).reshape(
        blocks, 2 * window_len, kv_local, HEAD_DIM
    )
    mark_band = banded(prev_marks, own_marks, window_len).astype(jnp.float32)
    query_marks = own_marks.reshape(blocks, window_len).astype(jnp.float32)
    query_blocks = queries.reshape(blocks, window_len, kv_local, group_size, HEAD_DIM)
    scores = jnp.einsum(
        "nqhgd,nkhd->nhgqk", query_blocks, key_band, preferred_element_type=jnp.float32
    ) * HEAD_DIM ** (-0.5)
    offsets = jnp.arange(window_len)[:, None] + window_len - jnp.arange(2 * window_len)[None, :]
    allowed = (
        (offsets >= 0) & (offsets < window_len) & (query_marks[:, :, None] == mark_band[:, None, :])
    )
    sink_logits = sinks.reshape(kv_local, group_size)[None, :, :, None]
    masked = jnp.where(allowed[:, None, None], scores, -jnp.inf)
    top_score = jnp.maximum(jnp.max(masked, axis=-1), sink_logits)
    exp_terms = jnp.where(allowed[:, None, None], jnp.exp(scores - top_score[..., None]), 0.0)
    denominator = jnp.sum(exp_terms, axis=-1) + jnp.exp(sink_logits - top_score)
    probabilities = (exp_terms / denominator[..., None]).astype(jnp.bfloat16)
    attended = jnp.einsum(
        "nhgqk,nkhd->nqhgd", probabilities, value_band, preferred_element_type=jnp.float32
    )
    attended = attended.astype(jnp.bfloat16).reshape(rows_here, head_local * HEAD_DIM)
    partial_value = jnp.dot(attended, out_weight, preferred_element_type=jnp.float32)
    col_width = model_width // tp_count
    col_start = tp_index * col_width
    share_sum = sent_and_summed(partial_value.astype(jnp.bfloat16), "tp", 1)
    residual_cols = lax.dynamic_slice_in_dim(residual, col_start, col_width, 1)
    updated_cols = (residual_cols.astype(jnp.float32) + share_sum).astype(jnp.bfloat16)
    cols_f32 = updated_cols.astype(jnp.float32)
    squares = lax.psum(jnp.sum(cols_f32 * cols_f32, axis=-1), "tp")
    inv_rms = lax.rsqrt(squares / model_width + epsilon)
    gain_cols = lax.dynamic_slice_in_dim(norm_gain, col_start, col_width, 0)
    normed_cols = (cols_f32 * inv_rms[:, None] * gain_cols).astype(jnp.bfloat16)
    normed = collect(normed_cols, "tp", 1)
    shared_pre = jnp.dot(normed, shared_gate, preferred_element_type=jnp.float32)
    shared_lin = jnp.dot(normed, shared_up, preferred_element_type=jnp.float32)
    shared_act = (jax.nn.silu(shared_pre) * shared_lin).astype(jnp.bfloat16)
    top_count = routes.shape[1]
    experts = lax.axis_size(SP)
    capacity = 2 * rows_here * top_count // experts
    flat_ids = routes.reshape(-1)
    one_hot = (flat_ids[:, None] == jnp.arange(experts, dtype=jnp.int32)[None, :]).astype(jnp.int32)
    rank_in = jnp.cumsum(one_hot, axis=0) - one_hot
    slot_dest = flat_ids * capacity + jnp.sum(rank_in * one_hot, axis=1)
    token_of = jnp.arange(rows_here * top_count, dtype=jnp.int32) // top_count
    slot_token = jnp.full((experts * capacity,), -1, jnp.int32).at[slot_dest].set(token_of)
    filled = slot_token >= 0
    safe_token = jnp.where(filled, slot_token, 0)
    outgoing = jnp.where(filled[:, None], normed_cols[safe_token], jnp.zeros((), jnp.bfloat16))
    pieces = two_step_exchange(
        outgoing.reshape(experts, capacity, col_width), ("sp_0", "sp_1"), (1, 0), 0, 0
    )
    arrived = lax.all_gather(pieces, "tp", axis=2, tiled=True)
    expert_rows = arrived.reshape(-1, model_width)
    gate_pre = jnp.dot(expert_rows, expert_gate[0], preferred_element_type=jnp.float32)
    up_lin = jnp.dot(expert_rows, expert_up[0], preferred_element_type=jnp.float32)
    expert_act = (jax.nn.silu(gate_pre) * up_lin).astype(jnp.bfloat16)
    gathered_expert, gathered_shared = sent_together((expert_act, shared_act), "tp", 1, 0)
    expert_out = jnp.dot(
        gathered_expert, expert_down[0], preferred_element_type=jnp.float32
    ).astype(jnp.bfloat16)
    returned = lax.all_to_all(
        expert_out.reshape(experts, capacity, col_width),
        SP,
        split_axis=0,
        concat_axis=0,
        tiled=True,
    )
    returned = returned.reshape(experts * capacity, col_width)
    picked = returned[slot_dest].astype(jnp.float32).reshape(rows_here, top_count, col_width)
    routed = jnp.sum(picked * route_weight[:, :, None], axis=1)
    shared_cols = jnp.dot(gathered_shared, shared_down, preferred_element_type=jnp.float32)
    return (updated_cols.astype(jnp.float32) + shared_cols + routed).astype(jnp.bfloat16)


def solution(mesh):
    torus = Mesh(
        mesh.devices.reshape(mesh.shape["grp"], 16, 2, mesh.shape["tp"]),
        ("grp", "sp_0", "sp_1", "tp"),
    )
    in_specs = (
        P(GRP_SP, None),
        P(GRP_SP, "tp"),
        P(GRP_SP, "tp"),
        P(GRP_SP, "tp"),
        P(GRP_SP),
        P(GRP_SP, None),
        P(GRP_SP, None),
        P("tp"),
        P("tp", None),
        P(),
        P(SP, None, "tp"),
        P(SP, None, "tp"),
        P(SP, None, "tp"),
        P(None, "tp"),
        P(None, "tp"),
        P(None, "tp"),
    )
    out_specs = P(GRP_SP, "tp")
    return jax.shard_map(
        shards, mesh=torus, in_specs=in_specs, out_specs=out_specs, check_vma=False
    )
```

profile of v0, /device:TPU:65, one launch (start us, length us, event | category | flops | bytes accessed | tf_op | source)
XLA Modules:
  0.0 356.7 jit_solution(9728244078039882902)
XLA Ops:
  6.6 0.7 bitcast_convert_fusion
  7.3 7.1 %collective-permute-start.1 = (bf16[128]{0:T(256)(128)(2,1)S(1)}, bf16[128]{0:T(256)(128)(2,1)S(1)}, u32[]{:S(2)}, u32[]{:S(2)}) collective-permute-start(bf16[128]{0:T(256)(128)(2,1)S(1)} %slice.57), channel_id=1, source_target_pairs={{0,8},{8,16},{16,24},{24,32},{32,40},{40,48},{48,56},{56,64},{64,7... | collective-permute-start | bytes 776 | tf_op jit(solution)/shard_map/ppermute | solution.py:17
  14.4 0.7 slice.60
  15.1 1.9 collective-permute-start.2
  17.0 0.7 slice.53
  17.8 6.1 %collective-permute-start = (bf16[128,64]{0,1:T(8,128)(2,1)S(1)}, bf16[128,64]{0,1:T(8,128)(2,1)S(1)}, u32[]{:S(2)}, u32[]{:S(2)}) collective-permute-start(bf16[128,64]{0,1:T(8,128)(2,1)S(1)} %slice.53), channel_id=1, source_target_pairs={{0,8},{8,16},{16,24},{24,32},{32,40},{40,48},{48,56},{56,64},{64,7... | collective-permute-start | bytes 49160 | tf_op jit(solution)/shard_map/ppermute | solution.py:17
  23.9 0.8 copy_bitcast_fusion
  24.7 0.8 copy_bitcast_fusion.2
  25.5 0.9 reshape.250
  26.4 24.3 %collective-permute-done.1 = bf16[128]{0:T(256)(128)(2,1)S(1)} collective-permute-done((bf16[128]{0:T(256)(128)(2,1)S(1)}, bf16[128]{0:T(256)(128)(2,1)S(1)}, u32[]{:S(2)}, u32[]{:S(2)}) %collective-permute-start.1) | collective-permute-done | bytes 288 | tf_op jit(solution)/shard_map/ppermute | solution.py:17
  50.7 0.1 compare_and_fusion
  50.8 1.9 collective-permute-done.2
  52.7 0.7 copy_bitcast_fusion.1
  53.5 0.3 select_reduce_fusion
  53.7 0.7 broadcast_maximum_fusion
  54.5 0.1 fusion.16
  54.6 0.7 exponential_add_fusion
  55.3 0.7 copy_bitcast_fusion.3
  56.1 0.3 fusion.10
  56.3 0.1 copy.41
  56.4 0.5 convolution_convert_fusion
  56.9 1.1 copy.79
  57.9 3.8 %all-to-all-start = ((bf16[8,256,256]{2,1,0:T(8,128)(2,1)}), bf16[8,256,256]{2,1,0:T(8,128)(2,1)S(1)}, u32[]{:S(2)}, u32[]{:S(2)}) async-start(bf16[8,256,256]{2,1,0:T(8,128)(2,1)} %bitcast.106), calls=%async_computation | async-start | bytes 2097152 | tf_op jit(solution)/shard_map/all_to_all | solution.py:28
  61.7 0.1 all-gather.3.cloned.1.call-start
  61.8 0.1 copy.44
  61.9 0.1 eq.47
  62.1 0.1 eq.51
  62.2 0.1 copy.43
  62.4 0.1 mul.82
  62.5 1.2 reduce-window.6
  63.7 0.2 slice_reduce_fusion
  64.0 0.1 fusion.29
  64.1 2.4 scatter_custom_fusion
  66.6 0.1 broadcast_in_dim.66
  66.7 0.8 dynamic_slice.7
  67.4 19.8 %all-to-all-done = bf16[8,256,256]{2,1,0:T(8,128)(2,1)S(1)} async-done(((bf16[8,256,256]{2,1,0:T(8,128)(2,1)}), bf16[8,256,256]{2,1,0:T(8,128)(2,1)S(1)}, u32[]{:S(2)}, u32[]{:S(2)}) %all-to-all-start) | async-done | bytes 1048608 | tf_op jit(solution)/shard_map/all_to_all | solution.py:28
  87.2 0.1 convert_reduce_fusion
  87.4 1.0 fusion.17
  88.4 11.1 %psum.7 = f32[256]{0:T(256)S(1)} all-reduce(f32[256]{0:T(256)S(1)} %get-tuple-element.5), channel_id=1, replica_groups=mesh['grp'=2,'sp_0'=16,'sp_1'=2,'tp'=8] {'tp'}, use_global_device_ids=true, to_apply=%region_8.9 | all-reduce | flops 256 | bytes 2048 | tf_op jit(solution)/shard_map/psum | solution.py:150
  99.5 0.1 fusion.19
  99.6 3.9 %gather_fusion = bf16[1024,256]{1,0:T(8,128)(2,1)S(1)} fusion(bf16[256,256]{1,0:T(8,128)(2,1)S(1)} %fusion.19, s32[1024]{0:T(1024)S(1)} %fusion.37), kind=kCustom, calls=%fused_computation | custom fusion | bytes 1052672 | tf_op jit(solution)/shard_map/gather | solution.py:169
  103.5 0.2 copy_select_fusion
  103.8 11.5 %all_to_all.25 = bf16[16,2,1,32,256]{4,3,0,2,1:T(8,128)(2,1)S(1)} all-to-all(bf16[16,2,1,32,256]{4,3,0,2,1:T(8,128)(2,1)S(1)} %copy_select_fusion), channel_id=1, replica_groups=mesh['grp'=2,'sp_0'=16,'sp_1'=2,'tp'=8] {'sp_1'}, dimensions={1} | all-to-all | bytes 1048576 | tf_op jit(solution)/shard_map/all_to_all | solution.py:54
  115.3 36.5 %all_to_all.26 = bf16[16,2,1,32,256]{4,3,1,2,0:T(8,128)(2,1)} all-to-all(bf16[16,2,1,32,256]{4,3,1,2,0:T(8,128)(2,1)S(1)} %copy.49), channel_id=1, replica_groups=mesh['grp'=2,'sp_0'=16,'sp_1'=2,'tp'=8] {'sp_0'}, dimensions={0} | all-to-all | bytes 1048576 | tf_op jit(solution)/shard_map/all_to_all | solution.py:54
  151.8 0.1 all-gather.3.cloned.1.call-update
  151.9 0.1 all-gather.5.cloned.1.call-start
  152.0 0.1 copy.50
  152.1 0.1 broadcast_in_dim.70
  152.2 24.5 %all_to_all.27 = bf16[8,256,256]{1,2,0:T(8,128)(2,1)S(1)} all-to-all(bf16[8,256,256]{1,2,0:T(8,128)(2,1)S(1)} %broadcast_in_dim.70), channel_id=1, replica_groups=mesh['grp'=2,'sp_0'=16,'sp_1'=2,'tp'=8] {'tp'}, dimensions={0} | all-to-all | bytes 2097152 | tf_op jit(solution)/shard_map/all_to_all | solution.py:34
  176.6 0.5 fusion.50
  177.1 0.5 fusion.9
  177.6 47.7 %all-gather.3.cloned.1.call-done = bf16[32,32,2048]{2,1,0:T(8,128)(2,1)} async-done(((bf16[32,32,256]{2,1,0:T(8,128)(2,1)}), bf16[32,32,2048]{2,1,0:T(8,128)(2,1)}) %all-gather.3.cloned.1.call-update) | async-done | bytes 4194320 | tf_op jit(solution)/shard_map/all_gather | solution.py:173
  225.3 3.6 %fusion.14 = f32[1024,128]{1,0:T(8,128)S(1)} fusion(bf16[1024,2048]{1,0:T(8,128)(2,1)} %bitcast.108, bf16[1,2048,128]{2,1,0:T(8,128)(2,1)S(1)} %copy-done.2), kind=kOutput, calls=%fused_computation.23 | convolution fusion | flops 536870912 | bytes 5242880 | tf_op jit(solution)/shard_map/dot_general | solution.py:175
  229.0 1.2 fusion.6
  230.2 0.7 pad_maximum_fusion
  231.0 59.2 %all-gather.5.cloned.1.call-done = bf16[1280,1024]{1,0:T(8,128)(2,1)} async-done(((bf16[1280,128]{1,0:T(8,128)(2,1)}), bf16[1280,1024]{1,0:T(8,128)(2,1)}) %all-gather.5.cloned.1.call-update) | async-done | bytes 2621456 | tf_op jit(solution)/shard_map/all_gather | solution.py:70
  290.2 3.1 fusion.2
  293.3 18.3 %all-to-all-start.4 = ((bf16[32,32,256]{2,1,0:T(8,128)(2,1)}), bf16[32,32,256]{2,1,0:T(8,128)(2,1)S(1)}, u32[]{:S(2)}, u32[]{:S(2)}) async-start(bf16[32,32,256]{2,1,0:T(8,128)(2,1)} %bitcast.25), calls=%async_computation.4 | async-start | bytes 1048576 | tf_op jit(solution)/shard_map/all_to_all | solution.py:182
  311.7 0.1 copy.51
  311.8 33.1 %all-to-all-done.4 = bf16[32,32,256]{2,1,0:T(8,128)(2,1)S(1)} async-done(((bf16[32,32,256]{2,1,0:T(8,128)(2,1)}), bf16[32,32,256]{2,1,0:T(8,128)(2,1)S(1)}, u32[]{:S(2)}, u32[]{:S(2)}) %all-to-all-start.4) | async-done | bytes 524320 | tf_op jit(solution)/shard_map/all_to_all | solution.py:182
  344.9 1.9 gather_fusion.1
  346.9 0.3 reshape.222
  347.2 0.7 multiply_reduce_fusion
  347.9 2.0 fusion.8
  (40 shorter events, 0.3 us)
Async XLA Ops:
  6.5 49.8 %copy-start = (bf16[128,2048]{1,0:T(8,128)(2,1)S(1)}, bf16[128,2048]{1,0:T(8,128)(2,1)}, u32[]{:S(2)}) copy-start(bf16[128,2048]{1,0:T(8,128)(2,1)} %param.24) | copy-start | bytes 1572868
  7.3 43.4 %collective-permute-start.1 = (bf16[128]{0:T(256)(128)(2,1)S(1)}, bf16[128]{0:T(256)(128)(2,1)S(1)}, u32[]{:S(2)}, u32[]{:S(2)}) collective-permute-start(bf16[128]{0:T(256)(128)(2,1)S(1)} %slice.57), channel_id=1, source_target_pairs={{0,8},{8,16},{16,24},{24,32},{32,40},{40,48},{48,56},{56,64},{64,7... | collective-permute-start | bytes 776 | tf_op jit(solution)/shard_map/ppermute | solution.py:17
  15.1 37.6 %collective-permute-start.2 = (bf16[128,64]{0,1:T(8,128)(2,1)S(1)}, bf16[128,64]{0,1:T(8,128)(2,1)S(1)}, u32[]{:S(2)}, u32[]{:S(2)}) collective-permute-start(bf16[128,64]{0,1:T(8,128)(2,1)S(1)} %slice.60), channel_id=1, source_target_pairs={{0,8},{8,16},{16,24},{24,32},{32,40},{40,48},{48,56},{56,64},{64,7... | collective-permute-start | bytes 49160 | tf_op jit(solution)/shard_map/ppermute | solution.py:17
  17.8 37.6 %collective-permute-start = (bf16[128,64]{0,1:T(8,128)(2,1)S(1)}, bf16[128,64]{0,1:T(8,128)(2,1)S(1)}, u32[]{:S(2)}, u32[]{:S(2)}) collective-permute-start(bf16[128,64]{0,1:T(8,128)(2,1)S(1)} %slice.53), channel_id=1, source_target_pairs={{0,8},{8,16},{16,24},{24,32},{32,40},{40,48},{48,56},{56,64},{64,7... | collective-permute-start | bytes 49160 | tf_op jit(solution)/shard_map/ppermute | solution.py:17
  56.4 5.4 %copy-start.5 = (s32[256,2]{0,1:T(2,128)S(1)}, s32[256,2]{0,1:T(2,128)}, u32[]{:S(2)}) copy-start(s32[256,2]{0,1:T(2,128)} %param.21) | copy-start | bytes 6148
  57.9 29.3 %all-to-all-start = ((bf16[8,256,256]{2,1,0:T(8,128)(2,1)}), bf16[8,256,256]{2,1,0:T(8,128)(2,1)S(1)}, u32[]{:S(2)}, u32[]{:S(2)}) async-start(bf16[8,256,256]{2,1,0:T(8,128)(2,1)} %bitcast.106), calls=%async_computation | async-start | bytes 2097152 | tf_op jit(solution)/shard_map/all_to_all | solution.py:28
  61.7 163.6 %all-gather.3.cloned.1.call-start = ((), (), s32[]{:S(2)}) async-start(), calls=%async_computation.5 | async-start | bytes 4718592 | tf_op jit(solution)/shard_map/all_gather | solution.py:173
  115.3 61.3 %copy-start.4 = (bf16[2048,128]{1,0:T(8,128)(2,1)S(1)}, bf16[2048,128]{1,0:T(8,128)(2,1)}, u32[]{:S(2)}) copy-start(bf16[2048,128]{1,0:T(8,128)(2,1)} %param.29) | copy-start | bytes 1572868
  151.9 25.2 %copy-start.7 = (bf16[2048,128]{1,0:T(8,128)(2,1)S(1)}, bf16[2048,128]{1,0:T(8,128)(2,1)}, u32[]{:S(2)}) copy-start(bf16[2048,128]{1,0:T(8,128)(2,1)} %param.30) | copy-start | bytes 1572868
  151.9 138.3 %all-gather.5.cloned.1.call-start = ((), (), s32[]{:S(2)}) async-start(), calls=%async_computation.6 | async-start | bytes 2949120 | tf_op jit(solution)/shard_map/all_gather | solution.py:70
  152.1 73.2 %copy-start.2 = (bf16[1,2048,128]{2,1,0:T(8,128)(2,1)S(1)}, bf16[1,2048,128]{2,1,0:T(8,128)(2,1)}, u32[]{:S(2)}) copy-start(bf16[1,2048,128]{2,1,0:T(8,128)(2,1)} %param.26) | copy-start | bytes 1572868
  225.3 3.6 %copy-start.1 = (bf16[32,32,2048]{2,1,0:T(8,128)(2,1)S(1)}, bf16[32,32,2048]{2,1,0:T(8,128)(2,1)}, u32[]{:S(2)}) copy-start(bf16[32,32,2048]{2,1,0:T(8,128)(2,1)} %all-gather.3.cloned.1.call-done) | copy-start | bytes 12582916
  225.3 3.6 %copy-start.8 = (bf16[1,2048,128]{2,1,0:T(8,128)(2,1)S(1)}, bf16[1,2048,128]{2,1,0:T(8,128)(2,1)}, u32[]{:S(2)}) copy-start(bf16[1,2048,128]{2,1,0:T(8,128)(2,1)} %param.27) | copy-start | bytes 1572868
  229.0 61.2 %copy-start.9 = (bf16[1,1024,256]{2,1,0:T(8,128)(2,1)S(1)}, bf16[1,1024,256]{2,1,0:T(8,128)(2,1)}, u32[]{:S(2)}) copy-start(bf16[1,1024,256]{2,1,0:T(8,128)(2,1)} %param.28) | copy-start | bytes 1572868
  231.0 80.6 %copy-start.6 = (f32[256,2]{0,1:T(2,128)S(1)}, f32[256,2]{0,1:T(2,128)}, u32[]{:S(2)}) copy-start(f32[256,2]{0,1:T(2,128)} %param.22) | copy-start | bytes 6148
  293.3 54.6 %copy-start.3 = (bf16[1024,256]{1,0:T(8,128)(2,1)S(1)}, bf16[1024,256]{1,0:T(8,128)(2,1)}, u32[]{:S(2)}) copy-start(bf16[1024,256]{1,0:T(8,128)(2,1)} %param.31) | copy-start | bytes 1572868
  293.3 51.6 %all-to-all-start.4 = ((bf16[32,32,256]{2,1,0:T(8,128)(2,1)}), bf16[32,32,256]{2,1,0:T(8,128)(2,1)S(1)}, u32[]{:S(2)}, u32[]{:S(2)}) async-start(bf16[32,32,256]{2,1,0:T(8,128)(2,1)} %bitcast.25), calls=%async_computation.4 | async-start | bytes 1048576 | tf_op jit(solution)/shard_map/all_to_all | solution.py:182
Sparse Core Ops, SparseCore 0:
  152.0 73.2 all-gather.2
  231.1 59.0 all-gather.4
where the time goes:
time: 358 us; the launch traced here: 357 us
  waiting for transfers between devices  186 us (52%)
  blocking collectives  83.5 us (23%)
  starting transfers between devices  37.3 us (10%)
  local copies, waits for them, and re-layouts  15.8 us (4%)
  between operations  13.8 us (4%)
  matrix products  11.9 us (3%)
  other arithmetic  8.26 us (2%)
    all_gather x1, waiting for transfers between devices, sent_together(): lax.all_gather(both, axis, axis=dim, tiled=True)  59.2 us
    all_to_all x2, blocking collectives, moved_by_axis(): lax.all_to_all(blocks, axes[k], split_axis=k, concat_axis=k, tiled=True)  48 us
    all_gather x1, waiting for transfers between devices, shards(): arrived = lax.all_gather(pieces, 'tp', axis=2, tiled=True)  47.7 us
    all_to_all x1, waiting for transfers between devices, shards(): lax.all_to_all(expert_out.reshape(experts, capacity, col_width), SP, spli...  33.1 us
    ppermute x3, waiting for transfers between devices, passed_along(): lax.ppermute(value, axis, [(source, source + steps) for source in range(l...  26.1 us
    all_to_all x1, blocking collectives, sent_to_all(): lax.all_to_all(jnp.broadcast_to(array[None], (size, *array.shape)), axis,...  24.5 us
    all_to_all x1, waiting for transfers between devices, sent_and_summed(): blocks = lax.all_to_all(split_up(array, dim, size), axis, 0, 0, tiled=True)  19.8 us
    all_to_all x1, starting transfers between devices, shards(): lax.all_to_all(expert_out.reshape(experts, capacity, col_width), SP, spli...  18.3 us
  transfers between devices with their start and end apart: 7, of which 6 were waited for; matrix products, arithmetic and copies ran while one was open for 4% of the time, Pallas kernels for 0%

commit v1 on v0

--- a/solution.py
+++ b/solution.py
@@ -170,7 +170,19 @@
     pieces = two_step_exchange(
         outgoing.reshape(experts, capacity, col_width), ("sp_0", "sp_1"), (1, 0), 0, 0
     )
-    arrived = lax.all_gather(pieces, "tp", axis=2, tiled=True)
+
+    def serve_joints(row_dim, packet):
+        parts_n = lax.axis_size("tp")
+        store = tuple((parts_n if b == row_dim else 1 for b in range(packet.ndim)))
+        return lax.all_to_all(
+            jnp.tile(packet, store),
+            axis_name="tp",
+            split_axis=row_dim,
+            concat_axis=row_dim,
+            tiled=True,
+        )
+
+    arrived = serve_joints(2, pieces)
     expert_rows = arrived.reshape(-1, model_width)
     gate_pre = jnp.dot(expert_rows, expert_gate[0], preferred_element_type=jnp.float32)
     up_lin = jnp.dot(expert_rows, expert_up[0], preferred_element_type=jnp.float32)

time: 358 us -> 445 us (1.24)
  blocking collectives: 83.5 us -> 22.6 us
  waiting for transfers between devices: 186 us -> 246 us
  local copies, waits for them, and re-layouts: 15.8 us -> 75.4 us
  starting transfers between devices: 37.3 us -> 62.2 us
    all_to_all x0 -> x3, waiting for transfers between devices: none -> 107 us  [the longest x1 84.4 us: serve_joints(): lax.all_to_all(jnp.tile(packet, store), axis_name='tp', split_axis=row_di...]
    all_gather x1 -> x0, waiting for transfers between devices: 47.7 us -> none  [shards(): arrived = lax.all_gather(pieces, 'tp', axis=2, tiled=True)]
    all_to_all x2 -> x1, blocking collectives: 48 us -> 11.5 us  [moved_by_axis(): lax.all_to_all(blocks, axes[k], split_axis=k, concat_axis=k, tiled=True)]
    unnamed x22 -> x26, local copies, waits for them, and re-layouts: 0.32 us -> 31.5 us
    all_to_all x0 -> x3, starting transfers between devices: none -> 24.9 us  [the longest x1 13.9 us: moved_by_axis(): lax.all_to_all(blocks, axes[k], split_axis=k, concat_axis=k, tiled=True)]
    all_to_all x1 -> x0, blocking collectives: 24.5 us -> none  [sent_to_all(): lax.all_to_all(jnp.broadcast_to(array[None], (size, *array.shape)), axis,...]
    all_to_all x0 -> x1, local copies, waits for them, and re-layouts: none -> 17.5 us  [serve_joints(): lax.all_to_all(jnp.tile(packet, store), axis_name='tp', split_axis=row_di...]
    another operation x2 -> x4, local copies, waits for them, and re-layouts: 0.94 us -> 10 us  [the longest x2 9.09 us: serve_joints(): jnp.tile(packet, store)]
  transfers between devices with their start and end apart: 7 -> 9, of which waited for: 6 -> 7; matrix products, arithmetic and copies ran while one was open for 4% -> 10% of each run, Pallas kernels for 0% -> 0%
where the time goes in v1:
time: 445 us; the launch traced here: 443 us
  waiting for transfers between devices  246 us (55%)
  local copies, waits for them, and re-layouts  75.4 us (17%)
  starting transfers between devices  62.2 us (14%)
  blocking collectives  22.6 us (5%)
  matrix products  14.4 us (3%)
  between operations  13.8 us (3%)
  other arithmetic  8.26 us (2%)
    all_to_all x1, waiting for transfers between devices, serve_joints(): lax.all_to_all(jnp.tile(packet, store), axis_name='tp', split_axis=row_di...  84.4 us
    all_gather x1, waiting for transfers between devices, sent_together(): lax.all_gather(both, axis, axis=dim, tiled=True)  60.1 us
    all_to_all x1, waiting for transfers between devices, shards(): lax.all_to_all(expert_out.reshape(experts, capacity, col_width), SP, spli...  33.1 us
    unnamed x26, local copies, waits for them, and re-layouts  31.5 us
    ppermute x3, waiting for transfers between devices, passed_along(): lax.ppermute(value, axis, [(source, source + steps) for source in range(l...  26.1 us
    all_to_all x1, waiting for transfers between devices, moved_by_axis(): lax.all_to_all(blocks, axes[k], split_axis=k, concat_axis=k, tiled=True)  22.4 us
    all_to_all x1, waiting for transfers between devices, sent_and_summed(): blocks = lax.all_to_all(split_up(array, dim, size), axis, 0, 0, tiled=True)  19.9 us
    all_to_all x1, starting transfers between devices, shards(): lax.all_to_all(expert_out.reshape(experts, capacity, col_width), SP, spli...  18.2 us
  transfers between devices with their start and end apart: 9, of which 7 were waited for; matrix products, arithmetic and copies ran while one was open for 10% of the time, Pallas kernels for 0%

profile of v1, /device:TPU:65, one launch (start us, length us, event | category | flops | bytes accessed | tf_op | source)
XLA Modules:
  0.0 442.7 jit_solution(1627293416514472309)
XLA Ops:
  6.6 0.7 bitcast_convert_fusion
  7.3 7.1 %collective-permute-start.1 = (bf16[128]{0:T(256)(128)(2,1)S(1)}, bf16[128]{0:T(256)(128)(2,1)S(1)}, u32[]{:S(2)}, u32[]{:S(2)}) collective-permute-start(bf16[128]{0:T(256)(128)(2,1)S(1)} %slice.57), channel_id=1, source_target_pairs={{0,8},{8,16},{16,24},{24,32},{32,40},{40,48},{48,56},{56,64},{64,7... | collective-permute-start | bytes 776 | tf_op jit(solution)/shard_map/ppermute | solution.py:17
  14.4 0.7 slice.60
  15.1 1.9 collective-permute-start.2
  17.0 0.7 slice.53
  17.8 6.1 %collective-permute-start = (bf16[128,64]{0,1:T(8,128)(2,1)S(1)}, bf16[128,64]{0,1:T(8,128)(2,1)S(1)}, u32[]{:S(2)}, u32[]{:S(2)}) collective-permute-start(bf16[128,64]{0,1:T(8,128)(2,1)S(1)} %slice.53), channel_id=1, source_target_pairs={{0,8},{8,16},{16,24},{24,32},{32,40},{40,48},{48,56},{56,64},{64,7... | collective-permute-start | bytes 49160 | tf_op jit(solution)/shard_map/ppermute | solution.py:17
  23.9 0.8 copy_bitcast_fusion
  24.7 0.8 copy_bitcast_fusion.2
  25.5 0.9 reshape.254
  26.4 24.3 %collective-permute-done.1 = bf16[128]{0:T(256)(128)(2,1)S(1)} collective-permute-done((bf16[128]{0:T(256)(128)(2,1)S(1)}, bf16[128]{0:T(256)(128)(2,1)S(1)}, u32[]{:S(2)}, u32[]{:S(2)}) %collective-permute-start.1) | collective-permute-done | bytes 288 | tf_op jit(solution)/shard_map/ppermute | solution.py:17
  50.7 0.1 compare_and_fusion
  50.8 1.9 collective-permute-done.2
  52.7 0.7 copy_bitcast_fusion.1
  53.5 0.3 select_reduce_fusion
  53.7 0.7 broadcast_maximum_fusion
  54.6 0.7 exponential_add_fusion
  55.3 0.7 copy_bitcast_fusion.3
  56.1 0.3 fusion.10
  56.4 0.5 convolution_convert_fusion
  56.9 1.1 copy.100
  57.9 3.8 all-to-all-start
  61.7 0.1 copy.63
  61.8 0.1 eq.47
  62.0 0.1 eq.51
  62.2 0.1 copy.62
  62.3 0.1 mul.82
  62.5 1.2 reduce-window.6
  63.6 0.2 slice_reduce_fusion
  64.0 2.4 scatter_custom_fusion
  66.6 0.8 dynamic_slice.7
  67.3 19.9 %all-to-all-done = bf16[8,256,256]{2,1,0:T(8,128)(2,1)S(1)} async-done(((bf16[8,256,256]{2,1,0:T(8,128)(2,1)}), bf16[8,256,256]{2,1,0:T(8,128)(2,1)S(1)}, u32[]{:S(2)}, u32[]{:S(2)}) %all-to-all-start) | async-done | bytes 1048608 | tf_op jit(solution)/shard_map/all_to_all | solution.py:28
  87.2 0.1 convert_reduce_fusion
  87.4 1.0 fusion.17
  88.4 11.1 %psum.7 = f32[256]{0:T(256)S(1)} all-reduce(f32[256]{0:T(256)S(1)} %get-tuple-element.5), channel_id=1, replica_groups=mesh['grp'=2,'sp_0'=16,'sp_1'=2,'tp'=8] {'tp'}, use_global_device_ids=true, to_apply=%region_8.9 | all-reduce | flops 256 | bytes 2048 | tf_op jit(solution)/shard_map/psum | solution.py:150
  99.6 3.9 gather_fusion
  103.5 0.2 copy_select_fusion
  103.7 11.5 %all_to_all.30 = bf16[16,2,1,32,256]{4,3,0,2,1:T(8,128)(2,1)S(1)} all-to-all(bf16[16,2,1,32,256]{4,3,0,2,1:T(8,128)(2,1)S(1)} %copy_select_fusion), channel_id=1, replica_groups=mesh['grp'=2,'sp_0'=16,'sp_1'=2,'tp'=8] {'sp_1'}, dimensions={1} | all-to-all | bytes 1048576 | tf_op jit(solution)/shard_map/all_to_all | solution.py:54
  115.2 0.8 copy.68
  116.1 13.9 %all-to-all-start.2 = ((bf16[16,2,1,32,256]{4,3,1,2,0:T(8,128)(2,1)}), bf16[16,2,1,32,256]{4,3,1,2,0:T(8,128)(2,1)S(1)}, u32[]{:S(2)}, u32[]{:S(2)}) async-start(bf16[16,2,1,32,256]{4,3,1,2,0:T(8,128)(2,1)} %copy.68), calls=%async_computation.2 | async-start | bytes 1048576 | tf_op jit(solution)/shard_map/all_to_all | solution.py:54
  130.1 22.4 %all-to-all-done.2 = bf16[16,2,1,32,256]{4,3,1,2,0:T(8,128)(2,1)S(1)} async-done(((bf16[16,2,1,32,256]{4,3,1,2,0:T(8,128)(2,1)}), bf16[16,2,1,32,256]{4,3,1,2,0:T(8,128)(2,1)S(1)}, u32[]{:S(2)}, u32[]{:S(2)}) %all-to-all-start.2) | async-done | bytes 524320 | tf_op jit(solution)/shard_map/all_to_all | solution.py:54
  152.5 1.0 broadcast_in_dim.70
  153.6 4.4 %all-to-all-start.4 = ((bf16[8,256,256]{1,2,0:T(8,128)(2,1)}), bf16[8,256,256]{1,2,0:T(8,128)(2,1)}, u32[]{:S(2)}, u32[]{:S(2)}) async-start(bf16[8,256,256]{1,2,0:T(8,128)(2,1)} %broadcast_in_dim.70), calls=%async_computation.4 | async-start | bytes 2097152 | tf_op jit(solution)/shard_map/all_to_all | solution.py:34
  158.0 3.0 copy.69
  161.0 6.1 %tile.11 = bf16[32,32,8,256]{1,0,3,2:T(8,128)(2,1)} broadcast(bf16[32,32,256]{1,0,2:T(8,128)(2,1)S(1)} %copy.69), dimensions={0,1,3} | broadcast | bytes 4718592 | tf_op jit(solution)/shard_map/tile | solution.py:178
  167.1 18.7 %reshape.258 = bf16[8,2,131072]{2,1,0:T(2,128)(2,1)} reshape(bf16[2048,32,32]{2,1,0:T(8,128)(2,1)} %bitcast.110) | data formatting | bytes 8388608
  185.8 6.6 %all-to-all-start.3 = ((bf16[8,2,131072]{2,1,0:T(2,128)(2,1)}), bf16[8,2,131072]{2,1,0:T(2,128)(2,1)}, u32[]{:S(2)}, u32[]{:S(2)}) async-start(bf16[8,2,131072]{2,1,0:T(2,128)(2,1)} %reshape.258), calls=%async_computation.3 | async-start | bytes 8388608 | tf_op jit(solution)/shard_map/all_to_all | solution.py:177
  192.4 0.2 all-gather.2.cloned.1.call-start
  192.7 1.7 fusion.50
  194.4 1.7 fusion.9
  196.1 84.4 %all-to-all-done.3 = bf16[8,2,131072]{2,1,0:T(2,128)(2,1)} async-done(((bf16[8,2,131072]{2,1,0:T(2,128)(2,1)}), bf16[8,2,131072]{2,1,0:T(2,128)(2,1)}, u32[]{:S(2)}, u32[]{:S(2)}) %all-to-all-start.3) | async-done | bytes 4194336 | tf_op jit(solution)/shard_map/all_to_all | solution.py:177
  280.5 12.4 %reshape.259 = bf16[2048,32,32]{2,1,0:T(8,128)(2,1)} reshape(bf16[8,2,131072]{2,1,0:T(2,128)(2,1)} %all-to-all-done.3) | data formatting | bytes 8388608
  292.9 17.5 %copy.70 = bf16[32,32,2048]{2,1,0:T(8,128)(2,1)} copy(bf16[32,32,2048]{1,0,2:T(8,128)(2,1)} %bitcast.111) | data formatting | bytes 8388608 | tf_op jit(solution)/shard_map/all_to_all | solution.py:177
  310.5 3.6 fusion.14
  314.1 1.3 fusion.6
  315.3 0.7 pad_maximum_fusion
  316.2 60.1 %all-gather.2.cloned.1.call-done = bf16[1280,1024]{1,0:T(8,128)(2,1)} async-done(((bf16[1280,128]{1,0:T(8,128)(2,1)}), bf16[1280,1024]{1,0:T(8,128)(2,1)}) %all-gather.2.cloned.1.call-update) | async-done | bytes 2621456 | tf_op jit(solution)/shard_map/all_gather | solution.py:70
  376.3 3.2 fusion.2
  379.5 18.2 %all-to-all-start.5 = ((bf16[32,32,256]{2,1,0:T(8,128)(2,1)}), bf16[32,32,256]{2,1,0:T(8,128)(2,1)S(1)}, u32[]{:S(2)}, u32[]{:S(2)}) async-start(bf16[32,32,256]{2,1,0:T(8,128)(2,1)} %bitcast.26), calls=%async_computation.5 | async-start | bytes 1048576 | tf_op jit(solution)/shard_map/all_to_all | solution.py:194
  397.7 0.1 copy.72
  397.8 33.1 %all-to-all-done.5 = bf16[32,32,256]{2,1,0:T(8,128)(2,1)S(1)} async-done(((bf16[32,32,256]{2,1,0:T(8,128)(2,1)}), bf16[32,32,256]{2,1,0:T(8,128)(2,1)S(1)}, u32[]{:S(2)}, u32[]{:S(2)}) %all-to-all-start.5) | async-done | bytes 524320 | tf_op jit(solution)/shard_map/all_to_all | solution.py:194
  430.9 1.9 gather_fusion.1
  432.9 0.3 reshape.226
  433.2 0.7 multiply_reduce_fusion
  433.9 2.0 fusion.8
  (48 shorter events, 0.9 us)
Async XLA Ops:
  6.5 49.8 %copy-start = (bf16[128,2048]{1,0:T(8,128)(2,1)S(1)}, bf16[128,2048]{1,0:T(8,128)(2,1)}, u32[]{:S(2)}) copy-start(bf16[128,2048]{1,0:T(8,128)(2,1)} %param.24) | copy-start | bytes 1572868
  7.3 43.4 %collective-permute-start.1 = (bf16[128]{0:T(256)(128)(2,1)S(1)}, bf16[128]{0:T(256)(128)(2,1)S(1)}, u32[]{:S(2)}, u32[]{:S(2)}) collective-permute-start(bf16[128]{0:T(256)(128)(2,1)S(1)} %slice.57), channel_id=1, source_target_pairs={{0,8},{8,16},{16,24},{24,32},{32,40},{40,48},{48,56},{56,64},{64,7... | collective-permute-start | bytes 776 | tf_op jit(solution)/shard_map/ppermute | solution.py:17
  15.1 37.6 %collective-permute-start.2 = (bf16[128,64]{0,1:T(8,128)(2,1)S(1)}, bf16[128,64]{0,1:T(8,128)(2,1)S(1)}, u32[]{:S(2)}, u32[]{:S(2)}) collective-permute-start(bf16[128,64]{0,1:T(8,128)(2,1)S(1)} %slice.60), channel_id=1, source_target_pairs={{0,8},{8,16},{16,24},{24,32},{32,40},{40,48},{48,56},{56,64},{64,7... | collective-permute-start | bytes 49160 | tf_op jit(solution)/shard_map/ppermute | solution.py:17
  17.8 37.6 %collective-permute-start = (bf16[128,64]{0,1:T(8,128)(2,1)S(1)}, bf16[128,64]{0,1:T(8,128)(2,1)S(1)}, u32[]{:S(2)}, u32[]{:S(2)}) collective-permute-start(bf16[128,64]{0,1:T(8,128)(2,1)S(1)} %slice.53), channel_id=1, source_target_pairs={{0,8},{8,16},{16,24},{24,32},{32,40},{40,48},{48,56},{56,64},{64,7... | collective-permute-start | bytes 49160 | tf_op jit(solution)/shard_map/ppermute | solution.py:17
  56.1 5.6 %copy-start.6 = (s32[256,2]{0,1:T(2,128)S(1)}, s32[256,2]{0,1:T(2,128)}, u32[]{:S(2)}) copy-start(s32[256,2]{0,1:T(2,128)} %param.21) | copy-start | bytes 6148
  57.9 29.3 %all-to-all-start = ((bf16[8,256,256]{2,1,0:T(8,128)(2,1)}), bf16[8,256,256]{2,1,0:T(8,128)(2,1)S(1)}, u32[]{:S(2)}, u32[]{:S(2)}) async-start(bf16[8,256,256]{2,1,0:T(8,128)(2,1)} %bitcast.109), calls=%async_computation | async-start | bytes 2097152 | tf_op jit(solution)/shard_map/all_to_all | solution.py:28
  116.1 36.5 %all-to-all-start.2 = ((bf16[16,2,1,32,256]{4,3,1,2,0:T(8,128)(2,1)}), bf16[16,2,1,32,256]{4,3,1,2,0:T(8,128)(2,1)S(1)}, u32[]{:S(2)}, u32[]{:S(2)}) async-start(bf16[16,2,1,32,256]{4,3,1,2,0:T(8,128)(2,1)} %copy.68), calls=%async_computation.2 | async-start | bytes 1048576 | tf_op jit(solution)/shard_map/all_to_all | solution.py:54
  153.6 32.3 %all-to-all-start.4 = ((bf16[8,256,256]{1,2,0:T(8,128)(2,1)}), bf16[8,256,256]{1,2,0:T(8,128)(2,1)}, u32[]{:S(2)}, u32[]{:S(2)}) async-start(bf16[8,256,256]{1,2,0:T(8,128)(2,1)} %broadcast_in_dim.70), calls=%async_computation.4 | async-start | bytes 2097152 | tf_op jit(solution)/shard_map/all_to_all | solution.py:34
  185.8 6.8 %copy-start.5 = (bf16[2048,128]{1,0:T(8,128)(2,1)S(1)}, bf16[2048,128]{1,0:T(8,128)(2,1)}, u32[]{:S(2)}) copy-start(bf16[2048,128]{1,0:T(8,128)(2,1)} %param.29) | copy-start | bytes 1572868
  185.8 8.5 %copy-start.8 = (bf16[2048,128]{1,0:T(8,128)(2,1)S(1)}, bf16[2048,128]{1,0:T(8,128)(2,1)}, u32[]{:S(2)}) copy-start(bf16[2048,128]{1,0:T(8,128)(2,1)} %param.30) | copy-start | bytes 1572868
  185.8 94.6 %all-to-all-start.3 = ((bf16[8,2,131072]{2,1,0:T(2,128)(2,1)}), bf16[8,2,131072]{2,1,0:T(2,128)(2,1)}, u32[]{:S(2)}, u32[]{:S(2)}) async-start(bf16[8,2,131072]{2,1,0:T(2,128)(2,1)} %reshape.258), calls=%async_computation.3 | async-start | bytes 8388608 | tf_op jit(solution)/shard_map/all_to_all | solution.py:177
  192.4 183.9 %all-gather.2.cloned.1.call-start = ((), (), s32[]{:S(2)}) async-start(), calls=%async_computation.6 | async-start | bytes 2949120 | tf_op jit(solution)/shard_map/all_gather | solution.py:70
  292.9 17.5 %copy-start.3 = (bf16[1,2048,128]{2,1,0:T(8,128)(2,1)S(1)}, bf16[1,2048,128]{2,1,0:T(8,128)(2,1)}, u32[]{:S(2)}) copy-start(bf16[1,2048,128]{2,1,0:T(8,128)(2,1)} %param.26) | copy-start | bytes 1572868
  310.4 3.6 copy-start.2
  310.4 3.6 copy-start.9
  314.1 62.2 %copy-start.10 = (bf16[1,1024,256]{2,1,0:T(8,128)(2,1)S(1)}, bf16[1,1024,256]{2,1,0:T(8,128)(2,1)}, u32[]{:S(2)}) copy-start(bf16[1,1024,256]{2,1,0:T(8,128)(2,1)} %param.28) | copy-start | bytes 1572868
  315.3 82.3 %copy-start.7 = (f32[256,2]{0,1:T(2,128)S(1)}, f32[256,2]{0,1:T(2,128)}, u32[]{:S(2)}) copy-start(f32[256,2]{0,1:T(2,128)} %param.22) | copy-start | bytes 6148
  316.1 117.7 %copy-start.4 = (bf16[1024,256]{1,0:T(8,128)(2,1)S(1)}, bf16[1024,256]{1,0:T(8,128)(2,1)}, u32[]{:S(2)}) copy-start(bf16[1024,256]{1,0:T(8,128)(2,1)} %param.31) | copy-start | bytes 1572868
  376.3 59.6 %copy-start.1 = (bf16[128,2048]{1,0:T(8,128)(2,1)S(1)}, bf16[128,2048]{1,0:T(8,128)(2,1)}, u32[]{:S(2)}) copy-start(bf16[128,2048]{1,0:T(8,128)(2,1)} %param.24) | copy-start | bytes 1572868
  379.5 51.5 %all-to-all-start.5 = ((bf16[32,32,256]{2,1,0:T(8,128)(2,1)}), bf16[32,32,256]{2,1,0:T(8,128)(2,1)S(1)}, u32[]{:S(2)}, u32[]{:S(2)}) async-start(bf16[32,32,256]{2,1,0:T(8,128)(2,1)} %bitcast.26), calls=%async_computation.5 | async-start | bytes 1048576 | tf_op jit(solution)/shard_map/all_to_all | solution.py:194
Sparse Core Ops, SparseCore 0:
  316.3 59.9 all-gather.1
